TPU v7x, 32 devices: a whole 2x2x4 slice. The times are simulated.
32 devices in a mesh: sp: 8 (over z, x), dp: 4 (over y, core).
Axes of the slice: x: 2, y: 2, z: 4, core: 2. Of those that a mesh axis runs over, the one named last changes fastest.
Arguments:
- queries: bfloat16 [16, 8, 512, 128], P('dp', None, 'sp'), may hold values from -6 to 6
- keys: bfloat16 [16, 8, 512, 128], P('dp', None, 'sp'), may hold values from -6 to 6
- values: bfloat16 [16, 8, 512, 128], P('dp', None, 'sp'), may hold values from -6 to 6
- input_gate: bfloat16 [16, 8, 512], P('dp', None, 'sp'), may hold values from -6 to 140
- forget_gate: bfloat16 [16, 8, 512], P('dp', None, 'sp'), may hold values from 0.5 to 11.5
- start_memory: float32 [16, 8, 128, 128], P('dp', None, 'sp'), may hold values from -6 to 6
- start_norm: float32 [16, 8, 128], P('dp', None, 'sp'), may hold values from -24 to 24
- start_level: float32 [16, 8], P('dp'), may hold values from 2 to 4
- head_gain: float32 [8, 128], replicated, may hold values from 0.1 to 1.9
- out_weight: bfloat16 [1024, 4096], P(None, 'dp'), may hold values from -0.1875 to 0.1875
Outputs:
- mixed: bfloat16 [16, 512, 4096], P('dp', 'sp')
All inputs are finite; a program needn't handle non-finite values.
Results may differ from a plain program's by a relative error of at most 0.019.
Values may be sent and summed in bfloat16 or wider, within the bound.
No kernel may reach another device: no remote copies, remote signals or barrier semaphores. Data moves between devices by JAX's collectives and lax.ppermute only.
A program may use at most 64 MiB of HBM per device.

v0:
```python
import jax
import jax.numpy as jnp
from jax import lax
from jax.sharding import PartitionSpec as P


negative_fill = -1e30
CHUNKS = 1


def send(tensor, axis, size, move):
    return lax.ppermute(tensor, axis, [(k, move(k)) for k in range(size)])


def gather_weight(weight, size):
    me = lax.axis_index("dp")
    width = weight.shape[1] // CHUNKS
    chunks = [weight[:, c * width : (c + 1) * width] for c in range(CHUNKS)]
    rounds = size // 2
    pieces = []
    for c in range(CHUNKS):
        pieces.append((me, c, chunks[c]))
    for c in range(CHUNKS):
        pieces.append((me ^ 1, c, send(chunks[c], "dp", size, lambda k: k ^ 1)))
    for step in range(1, rounds):
        for c in range(CHUNKS):
            far = send(chunks[c], "dp", size, lambda k: (k + 2 * step) % size)
            source = (me - 2 * step) % size
            pieces.append((source, c, far))
            pieces.append((source ^ 1, c, send(far, "dp", size, lambda k: k ^ 1)))
    return pieces, width


def gather_small(tensor, size):
    me = lax.axis_index("sp")
    whole = tensor[None]
    bit = 1
    while bit < size:
        other = send(whole, "sp", size, lambda k: k ^ bit)
        upper = (me & bit) != 0
        whole = jnp.concatenate(
            [jnp.where(upper, other, whole), jnp.where(upper, whole, other)], axis=0
        )
        bit *= 2
    return whole


def pick(tensor, index):
    return lax.dynamic_index_in_dim(tensor, index, 0, keepdims=False)


def cell(query, key_in, value, input_pre, forget_pre, memory, normal, level, size):
    count, length, head_width = query.shape
    rows = memory.shape[1]
    factor = head_width ** (-0.5)
    me = lax.axis_index("sp")
    side = me % 2
    pair = me // 2
    pairs = size // 2

    gate_in = input_pre.astype(jnp.float32)
    cumulative = jnp.cumsum(jax.nn.log_sigmoid(forget_pre.astype(jnp.float32)), axis=-1)
    total = cumulative[:, -1]
    weights_log = total[:, None] - cumulative + gate_in
    local_max = jnp.max(weights_log, axis=-1)
    weights = jnp.exp(weights_log - local_max[:, None])
    weighted = key_in.astype(jnp.float32) * weights[..., None]
    local_norm = jnp.sum(weighted, axis=1)
    small = jnp.concatenate(
        [local_norm, normal, total[:, None], local_max[:, None]], axis=1
    )
    added = jnp.einsum(
        "psd,pse->pde", weighted.astype(jnp.bfloat16), value, preferred_element_type=jnp.float32
    ).astype(jnp.bfloat16)
    groups = added.reshape(count, pairs, 2, rows, head_width)
    even = groups[:, :, 0]
    odd = groups[:, :, 1]
    first = side == 0
    kept = jnp.where(first, even, odd)
    given, small = lax.optimization_barrier((jnp.where(first, odd, even), small))
    partner = send(given, "sp", size, lambda k: k ^ 1)
    gathered = gather_small(small, size)
    low = jnp.where(first, kept, partner).astype(jnp.float32)
    high = jnp.where(first, partner, kept).astype(jnp.float32)

    norms = gathered[:, :, :head_width]
    start_normal = jnp.moveaxis(
        gathered[:, :, head_width : head_width + rows], 0, 1
    ).reshape(count, head_width)
    totals = jnp.cumsum(gathered[:, :, head_width + rows], axis=0)
    own_level = gathered[:, :, head_width + rows + 1] - totals
    after = jnp.maximum(lax.cummax(own_level, axis=0), level[None])
    before = jnp.concatenate([level[None], after[:-1]], axis=0)
    even_before = before[0::2]
    odd_after = after[1::2]

    low_scale = jnp.exp(pick(own_level, 2 * pair) - pick(odd_after, pair))
    high_scale = jnp.exp(pick(own_level, 2 * pair + 1) - pick(odd_after, pair))
    both = (
        low_scale[:, None, None, None] * low + high_scale[:, None, None, None] * high
    ).astype(jnp.bfloat16)
    both = jnp.swapaxes(both, 0, 1)
    arrived = [pick(both, pair)]
    for step in range(1, pairs):
        arrived.append(
            send(
                pick(both, (pair + step) % pairs),
                "sp",
                size,
                lambda k: (k + 2 * step) % size,
            )
        )
    states = []
    for step in range(pairs):
        target = (pair + step) % pairs
        frame = pick(even_before, target)
        state = jnp.exp(level - frame)[:, None, None] * memory
        for back in range(pairs):
            source = (pair - back) % pairs
            scale = jnp.where(
                source < target, jnp.exp(jnp.minimum(pick(odd_after, source) - frame, 0.0)), 0.0
            )
            state = state + scale[:, None, None] * arrived[back].astype(jnp.float32)
        states.append(state.astype(jnp.bfloat16))
    returned = [states[0]]
    for step in range(1, pairs):
        returned.append(send(states[step], "sp", size, lambda k: (k + 2 * step) % size))
    stacked = jnp.stack(returned[::-1] + returned[::-1], axis=0)
    ordered = lax.dynamic_slice_in_dim(stacked, pairs - 1 - pair, pairs, axis=0)
    ordered = jnp.swapaxes(ordered, 0, 1)
    mid_after = pick(after, 2 * pair)
    mid = (
        jnp.exp(pick(even_before, pair) - mid_after)[:, None, None, None]
        * ordered.astype(jnp.float32)
        + jnp.exp(pick(own_level, 2 * pair) - mid_after)[:, None, None, None] * low
    ).astype(jnp.bfloat16)
    mine = jnp.where(first, ordered, mid)
    other = send(jnp.where(first, mid, ordered), "sp", size, lambda k: k ^ 1)
    state = jnp.stack(
        [jnp.where(first, mine, other), jnp.where(first, other, mine)], axis=2
    ).reshape(count, head_width, head_width)

    frame = pick(before, me)
    stabilizer = frame + pick(totals, me) - total
    blocks = jnp.arange(size)[:, None]
    shares = jnp.where(blocks < me, jnp.exp(jnp.minimum(own_level - frame[None], 0.0)), 0.0)
    norm_state = jnp.exp(level - frame)[:, None] * start_normal + jnp.sum(
        shares[..., None] * norms, axis=0
    )

    causal = jnp.tril(jnp.ones((length, length), dtype=bool))
    logits = jnp.where(
        causal,
        cumulative[:, :, None] - cumulative[:, None, :] + gate_in[:, None, :],
        negative_fill,
    )
    carried = cumulative + stabilizer[:, None]
    running_max = jnp.maximum(carried, jnp.max(logits, axis=-1))
    raw = (
        jnp.einsum("ptd,psd->pts", query, key_in, preferred_element_type=jnp.float32) * factor
    )
    scores = raw * jnp.exp(logits - running_max[..., None])
    carry_weight = jnp.exp(carried - running_max) * factor
    inner = jnp.einsum(
        "pts,pse->pte", scores.astype(jnp.bfloat16), value, preferred_element_type=jnp.float32
    )
    denominator = jnp.sum(scores, axis=-1) + carry_weight * jnp.sum(
        query.astype(jnp.float32) * norm_state[:, None, :], axis=-1
    )
    numerator = inner + carry_weight[..., None] * jnp.einsum(
        "ptd,pde->pte", query, state, preferred_element_type=jnp.float32
    )
    return (numerator / jnp.maximum(jnp.abs(denominator), 1.0)[..., None]).astype(jnp.bfloat16)


def on_device(
    queries,
    keys,
    values,
    input_gate,
    forget_gate,
    start_memory,
    start_norm,
    start_level,
    head_gain,
    out_weight,
):
    local_seqs, heads, tokens_here, head_width = queries.shape
    count = local_seqs * heads
    pieces, width = gather_weight(out_weight, lax.axis_size("dp"))

    def to_items(tensor):
        return tensor.reshape((count,) + tensor.shape[2:])

    hidden = cell(
        to_items(queries),
        to_items(keys),
        to_items(values),
        to_items(input_gate),
        to_items(forget_gate),
        to_items(start_memory),
        to_items(start_norm),
        start_level.reshape(count),
        lax.axis_size("sp"),
    ).reshape(local_seqs, heads, tokens_here, head_width)
    normed = (hidden.astype(jnp.float32) * head_gain[:, None, :]).astype(jnp.bfloat16)
    flat = jnp.swapaxes(normed, 1, 2).reshape(local_seqs, tokens_here, heads * head_width)
    mixed = jnp.zeros(
        (local_seqs, tokens_here, out_weight.shape[1] * lax.axis_size("dp")), jnp.bfloat16
    )
    for block, chunk, piece in pieces:
        part = jnp.einsum("stf,fc->stc", flat, piece, preferred_element_type=jnp.float32)
        mixed = lax.dynamic_update_slice(
            mixed,
            part.astype(jnp.bfloat16),
            (0, 0, block * out_weight.shape[1] + chunk * width),
        )
    return mixed


def solution(mesh):
    in_specs = (
        P("dp", None, "sp", None),
        P("dp", None, "sp", None),
        P("dp", None, "sp", None),
        P("dp", None, "sp"),
        P("dp", None, "sp"),
        P("dp", None, "sp", None),
        P("dp", None, "sp"),
        P("dp", None),
        P(),
        P(None, "dp"),
    )
    out_specs = P("dp", "sp", None)

    return jax.shard_map(on_device, mesh=mesh, in_specs=in_specs, out_specs=out_specs, check_vma=False)
```

profile of v0, /device:TPU:0, one launch (start us, length us, event | category | flops | bytes accessed | tf_op | source)
XLA Modules:
  0.0 85.1 jit_solution(12685359666445709721)
XLA Ops:
  0.0 0.5 collective-permute-start.11
  0.5 2.6 %collective-permute-start.12 = (bf16[1024,1024]{1,0:T(8,128)(2,1)}, bf16[1024,1024]{1,0:T(8,128)(2,1)}, u32[]{:S(2)}, u32[]{:S(2)}) collective-permute-start(bf16[1024,1024]{1,0:T(8,128)(2,1)} %param.19), channel_id=1, source_target_pairs={{0,2},{1,3},{2,0},{3,1},{4,6},{5,7},{6,4},{7,5},{8,10},{9,11},{10,... | collective-permute-start | bytes 6291464 | tf_op jit(solution)/shard_map/ppermute | solution.py:12
  3.1 0.7 fusion.84
  3.8 0.2 reduce_window_sum.26
  4.0 0.2 fusion.120
  4.2 0.1 sub.298
  4.3 0.9 %fusion.93 = f32[4,8]{1,0:T(4,128)S(1)} fusion(bf16[4,8,64]{2,1,0:T(8,128)(2,1)} %param.13, f32[32,64]{1,0:T(8,128)S(1)} %reduce_window_sum.26, f32[4,8]{1,0:T(4,128)S(1)} %sub.298), kind=kLoop, calls=%fused_computation.157 | loop fusion | flops 8160 | bytes 12544 | tf_op jit(solution)/shard_map/reduce_max | solution.py:65
  5.1 0.1 sub.301
  5.2 0.8 subtract_exponential_fusion
  6.1 0.8 subtract_exponential_fusion.1
  6.9 1.4 %multiply_reduce_fusion.1 = f32[4,8,128]{2,1,0:T(8,128)S(1)} fusion(bf16[4,8,64,128]{3,2,1,0:T(8,128)(2,1)} %param.11, f32[4,8,64]{2,1,0:T(8,128)S(1)} %subtract_exponential_fusion), kind=kLoop, calls=%fused_computation.34 | loop fusion | flops 782336 | bytes 548864 | tf_op jit(solution)/shard_map/reduce_sum | solution.py:68
  8.3 2.2 %convolution_convert_fusion = bf16[32,128,128]{2,1,0:T(8,128)(2,1)S(1)} fusion(bf16[32,64,128]{2,1,0:T(8,128)(2,1)S(1)} %bitcast.207, bf16[32,64,128]{2,1,0:T(8,128)(2,1)} %bitcast.210, f32[32,64]{1,0:T(8,128)S(1)} %subtract_exponential_fusion.1), kind=kOutput, calls=%fused_computation.8 | convolution fusion | flops 68419584 | bytes 2105344 | tf_op jit(solution)/shard_map/psd,pse->pde/dot_general | solution.py:72
  10.5 0.1 select_bitcast_fusion.2
  10.6 0.9 %fusion.49 = bf16[32,4,16,128]{3,2,0,1:T(8,128)(2,1)} fusion(bf16[32,4,1,16,128]{4,3,2,1,0:T(8,128)(2,1)S(1)} %get-tuple-element.35, bf16[32,4,1,16,128]{4,3,2,1,0:T(8,128)(2,1)S(1)} %get-tuple-element.34, pred[]{:T(512)S(6)} %eq.29), kind=kLoop, calls=%fused_computation.46 | loop fusion | flops 262144 | bytes 1572865 | tf_op jit(solution)/shard_map/jit(_where)/select_n | solution.py:80
  11.5 0.1 pad_maximum_fusion.4
  11.6 1.5 %collective-permute-start = (f32[1,32,146]{2,1,0:T(8,128)S(1)}, f32[1,32,146]{2,1,0:T(8,128)S(1)}, u32[]{:S(2)}, u32[]{:S(2)}) collective-permute-start(f32[1,32,146]{2,1,0:T(8,128)S(1)} %bitcast.215), channel_id=1, source_target_pairs={{0,4},{4,0},{8,12},{12,8},{16,20},{20,16},{24,28},{28,24},{1,5},{5... | collective-permute-start | bytes 56072 | tf_op jit(solution)/shard_map/ppermute | solution.py:12
  13.1 0.5 collective-permute-start.3
  13.6 1.9 %collective-permute-done = f32[1,32,146]{2,1,0:T(8,128)S(1)} collective-permute-done((f32[1,32,146]{2,1,0:T(8,128)S(1)}, f32[1,32,146]{2,1,0:T(8,128)S(1)}, u32[]{:S(2)}, u32[]{:S(2)}) %collective-permute-start) | collective-permute-done | bytes 18720 | tf_op jit(solution)/shard_map/ppermute | solution.py:12
  15.5 1.6 %collective-permute-start.1 = (f32[2,32,146]{2,1,0:T(8,128)S(1)}, f32[2,32,146]{2,1,0:T(8,128)S(1)}, u32[]{:S(2)}, u32[]{:S(2)}) collective-permute-start(f32[2,32,146]{2,1,0:T(8,128)S(1)} %pad_maximum_fusion.3), channel_id=1, source_target_pairs={{0,8},{4,12},{8,0},{12,4},{16,24},{20,28},{24,16},{28,20},{1,9},{5... | collective-permute-start | bytes 112136 | tf_op jit(solution)/shard_map/ppermute | solution.py:12
  17.2 0.6 fusion.41
  17.8 0.1 max.45
  17.9 0.1 broadcast_in_dim_reshape.4
  18.2 1.7 %collective-permute-done.1 = f32[2,32,146]{2,1,0:T(8,128)S(1)} collective-permute-done((f32[2,32,146]{2,1,0:T(8,128)S(1)}, f32[2,32,146]{2,1,0:T(8,128)S(1)}, u32[]{:S(2)}, u32[]{:S(2)}) %collective-permute-start.1) | collective-permute-done | bytes 37408 | tf_op jit(solution)/shard_map/ppermute | solution.py:12
  19.9 2.7 %collective-permute-start.2 = (f32[4,32,146]{2,1,0:T(8,128)S(1)}, f32[4,32,146]{2,1,0:T(8,128)S(1)}, u32[]{:S(2)}, u32[]{:S(2)}) collective-permute-start(f32[4,32,146]{2,1,0:T(8,128)S(1)} %pad_maximum_fusion.2), channel_id=1, source_target_pairs={{0,16},{4,20},{8,24},{12,28},{16,0},{20,4},{24,8},{28,12},{1,17},{... | collective-permute-start | bytes 224264 | tf_op jit(solution)/shard_map/ppermute | solution.py:12
  22.5 5.2 %collective-permute-done.2 = f32[4,32,146]{2,1,0:T(8,128)S(1)} collective-permute-done((f32[4,32,146]{2,1,0:T(8,128)S(1)}, f32[4,32,146]{2,1,0:T(8,128)S(1)}, u32[]{:S(2)}, u32[]{:S(2)}) %collective-permute-start.2) | collective-permute-done | bytes 74784 | tf_op jit(solution)/shard_map/ppermute | solution.py:12
  27.7 0.3 fusion.92
  28.1 0.1 copy.67
  28.3 0.2 select_reduce_fusion
  28.5 0.1 fusion.83
  28.6 0.1 squeeze.84
  28.7 0.1 copy.57
  28.8 0.2 subtract_reduce_fusion
  29.2 0.1 copy.66
  29.3 0.1 reshape.549
  29.4 0.8 fusion.121
  30.2 0.3 fusion.40
  30.6 0.7 collective-permute-start.4
  31.3 3.4 %collective-permute-start.5 = (bf16[32,16,128]{2,1,0:T(8,128)(2,1)S(1)}, bf16[32,16,128]{2,1,0:T(8,128)(2,1)S(1)}, u32[]{:S(2)}, u32[]{:S(2)}) collective-permute-start(bf16[32,16,128]{2,1,0:T(8,128)(2,1)S(1)} %get-tuple-element.37), channel_id=1, source_target_pairs={{0,16},{4,20},{8,24},{12,28},{16,0},{20,4},{24,8},{28,12},{1,17},{... | collective-permute-start | bytes 393224 | tf_op jit(solution)/shard_map/ppermute | solution.py:12
  34.7 4.2 %collective-permute-done.4 = bf16[32,16,128]{2,1,0:T(8,128)(2,1)S(1)} collective-permute-done((bf16[32,16,128]{2,1,0:T(8,128)(2,1)S(1)}, bf16[32,16,128]{2,1,0:T(8,128)(2,1)S(1)}, u32[]{:S(2)}, u32[]{:S(2)}) %collective-permute-start.4) | collective-permute-done | bytes 131104 | tf_op jit(solution)/shard_map/ppermute | solution.py:12
  39.0 3.7 %collective-permute-done.5 = bf16[32,16,128]{2,1,0:T(8,128)(2,1)S(1)} collective-permute-done((bf16[32,16,128]{2,1,0:T(8,128)(2,1)S(1)}, bf16[32,16,128]{2,1,0:T(8,128)(2,1)S(1)}, u32[]{:S(2)}, u32[]{:S(2)}) %collective-permute-start.5) | collective-permute-done | bytes 131104 | tf_op jit(solution)/shard_map/ppermute | solution.py:12
  42.7 0.1 collective-permute-done.6
  42.8 0.4 fusion.68
  43.2 3.0 %collective-permute-start.7 = (bf16[32,16,128]{2,1,0:T(8,128)(2,1)S(1)}, bf16[32,16,128]{2,1,0:T(8,128)(2,1)S(1)}, u32[]{:S(2)}, u32[]{:S(2)}) collective-permute-start(bf16[32,16,128]{2,1,0:T(8,128)(2,1)S(1)} %get-tuple-element.32), channel_id=1, source_target_pairs={{0,24},{4,28},{8,0},{12,4},{16,8},{20,12},{24,16},{28,20},{1,25},{... | collective-permute-start | bytes 393224 | tf_op jit(solution)/shard_map/ppermute | solution.py:12
  46.2 0.4 fusion.72
  46.6 1.7 %collective-permute-start.8 = (bf16[32,16,128]{2,1,0:T(8,128)(2,1)S(1)}, bf16[32,16,128]{2,1,0:T(8,128)(2,1)S(1)}, u32[]{:S(2)}, u32[]{:S(2)}) collective-permute-start(bf16[32,16,128]{2,1,0:T(8,128)(2,1)S(1)} %get-tuple-element.30), channel_id=1, source_target_pairs={{0,16},{4,20},{8,24},{12,28},{16,0},{20,4},{24,8},{28,12},{1,17},{... | collective-permute-start | bytes 393224 | tf_op jit(solution)/shard_map/ppermute | solution.py:12
  48.3 1.9 %collective-permute-done.7 = bf16[32,16,128]{2,1,0:T(8,128)(2,1)S(1)} collective-permute-done((bf16[32,16,128]{2,1,0:T(8,128)(2,1)S(1)}, bf16[32,16,128]{2,1,0:T(8,128)(2,1)S(1)}, u32[]{:S(2)}, u32[]{:S(2)}) %collective-permute-start.7) | collective-permute-done | bytes 131104 | tf_op jit(solution)/shard_map/ppermute | solution.py:12
  50.2 9.6 %collective-permute-done.8 = bf16[32,16,128]{2,1,0:T(8,128)(2,1)S(1)} collective-permute-done((bf16[32,16,128]{2,1,0:T(8,128)(2,1)S(1)}, bf16[32,16,128]{2,1,0:T(8,128)(2,1)S(1)}, u32[]{:S(2)}, u32[]{:S(2)}) %collective-permute-start.8) | collective-permute-done | bytes 131104 | tf_op jit(solution)/shard_map/ppermute | solution.py:12
  60.0 0.4 fusion.42
  60.4 1.2 %collective-permute-start.10 = (bf16[32,4,16,128]{3,2,0,1:T(8,128)(2,1)S(1)}, bf16[32,4,16,128]{3,2,0,1:T(8,128)(2,1)S(1)}, u32[]{:S(2)}, u32[]{:S(2)}) collective-permute-start(bf16[32,4,16,128]{3,2,0,1:T(8,128)(2,1)S(1)} %fusion.42), channel_id=1, source_target_pairs={{0,4},{4,0},{8,12},{12,8},{16,20},{20,16},{24,28},{28,24},{1,5},{5... | collective-permute-start | bytes 1572872 | tf_op jit(solution)/shard_map/ppermute | solution.py:12
  61.6 0.3 multiply_reduce_fusion
  62.0 0.3 fusion.50
  62.4 0.1 fusion.87
  62.5 11.0 %collective-permute-done.10 = bf16[32,4,16,128]{3,2,0,1:T(8,128)(2,1)S(1)} collective-permute-done((bf16[32,4,16,128]{3,2,0,1:T(8,128)(2,1)S(1)}, bf16[32,4,16,128]{3,2,0,1:T(8,128)(2,1)S(1)}, u32[]{:S(2)}, u32[]{:S(2)}) %collective-permute-start.10) | collective-permute-done | bytes 524320 | tf_op jit(solution)/shard_map/ppermute | solution.py:12
  73.5 0.5 select_bitcast_fusion.1
  74.1 0.1 pad_maximum_fusion
  74.2 0.3 copy.65
  74.5 0.8 fusion.12
  75.3 0.2 broadcast_in_dim.36
  75.5 1.3 %copy-done.8 = bf16[1024,1024]{1,0:T(8,128)(2,1)S(1)} copy-done((bf16[1024,1024]{1,0:T(8,128)(2,1)S(1)}, bf16[1024,1024]{1,0:T(8,128)(2,1)}, u32[]{:S(2)}) %copy-start.8) | copy-done | bytes 2097176
  76.9 0.7 fusion.34
  77.6 2.3 %fusion.31 = bf16[4,64,4096]{2,1,0:T(8,128)(2,1)S(1)} fusion(bf16[4,64,4096]{2,1,0:T(8,128)(2,1)S(1)} %fusion.34, s32[]{:T(128)S(6)} %select_n.477, bf16[1024,1024]{1,0:T(8,128)(2,1)} %collective-permute-done.11, bf16[4,8,64,128]{3,2,1,0:T(8,128)(2,1)S(1)} %bitcast.221, f32[8,128]{1,0:T(8,128)S(1)} %copy-done.9), kind=kOutput, calls=%fused_computation.24 | convolution fusion | flops 537919488 | bytes 3149828 | tf_op jit(solution)/shard_map/stf,fc->stc/dot_general | solution.py:212
  79.9 2.3 %fusion.28 = bf16[4,64,4096]{2,1,0:T(8,128)(2,1)S(1)} fusion(bf16[4,64,4096]{2,1,0:T(8,128)(2,1)S(1)} %fusion.31, s32[]{:T(128)S(6)} %select_n.479, bf16[1024,1024]{1,0:T(8,128)(2,1)} %collective-permute-done.12, bf16[4,8,64,128]{3,2,1,0:T(8,128)(2,1)S(1)} %bitcast.222, f32[8,128]{1,0:T(8,128)S(1)} %copy-done.9), kind=kOutput, calls=%fused_computation.23 | convolution fusion | flops 537919488 | bytes 3149828 | tf_op jit(solution)/shard_map/stf,fc->stc/dot_general | solution.py:212
  82.2 1.3 %copy-done.1 = bf16[4,64,4096]{2,1,0:T(8,128)(2,1)} copy-done((bf16[4,64,4096]{2,1,0:T(8,128)(2,1)}, bf16[4,64,4096]{2,1,0:T(8,128)(2,1)S(1)}, u32[]{:S(2)}) %copy-start.1) | copy-done | bytes 2097176
  83.5 1.5 %fusion.25 = bf16[4,64,4096]{2,1,0:T(8,128)(2,1)} fusion(bf16[4,64,4096]{2,1,0:T(8,128)(2,1)} %copy-done.1, s32[]{:T(128)S(6)} %select_n.480, bf16[1024,1024]{1,0:T(8,128)(2,1)S(1)} %collective-permute-done.13, bf16[4,8,64,128]{3,2,1,0:T(8,128)(2,1)S(1)} %bitcast.223, f32[8,128]{1,0:T(8,128)S(1)} %copy-done.9), kind=kOutput, calls=%fused_computation.22 | convolution fusion | flops 537919488 | bytes 3149828 | tf_op jit(solution)/shard_map/stf,fc->stc/dot_general | solution.py:212
  (61 shorter events, 1.0 us)
Async XLA Ops:
  0.0 8.3 %copy-start = (bf16[4,8,64,128]{3,2,1,0:T(8,128)(2,1)S(1)}, bf16[4,8,64,128]{3,2,1,0:T(8,128)(2,1)}, u32[]{:S(2)}) copy-start(bf16[4,8,64,128]{3,2,1,0:T(8,128)(2,1)} %param.12) | copy-start | bytes 1572868
  0.0 77.6 %collective-permute-start.11 = (bf16[1024,1024]{1,0:T(8,128)(2,1)}, bf16[1024,1024]{1,0:T(8,128)(2,1)}, u32[]{:S(2)}, u32[]{:S(2)}) collective-permute-start(bf16[1024,1024]{1,0:T(8,128)(2,1)} %param.19), channel_id=1, source_target_pairs={{0,1},{1,0},{2,3},{3,2},{4,5},{5,4},{6,7},{7,6},{8,9},{9,8},{10,11... | collective-permute-start | bytes 6291464 | tf_op jit(solution)/shard_map/ppermute | solution.py:12
  0.5 61.8 %collective-permute-start.12 = (bf16[1024,1024]{1,0:T(8,128)(2,1)}, bf16[1024,1024]{1,0:T(8,128)(2,1)}, u32[]{:S(2)}, u32[]{:S(2)}) collective-permute-start(bf16[1024,1024]{1,0:T(8,128)(2,1)} %param.19), channel_id=1, source_target_pairs={{0,2},{1,3},{2,0},{3,1},{4,6},{5,7},{6,4},{7,5},{8,10},{9,11},{10,... | collective-permute-start | bytes 6291464 | tf_op jit(solution)/shard_map/ppermute | solution.py:12
  10.5 1.0 %copy-start.7 = (f32[4,8,16]{2,1,0:T(8,128)S(1)}, f32[4,8,16]{2,1,0:T(8,128)}, u32[]{:S(2)}) copy-start(f32[4,8,16]{2,1,0:T(8,128)} %param.16) | copy-start | bytes 6148
  10.5 3.1 %copy-start.5 = (bf16[4,8,64]{2,1,0:T(8,128)(2,1)S(1)}, bf16[4,8,64]{2,1,0:T(8,128)(2,1)}, u32[]{:S(2)}) copy-start(bf16[4,8,64]{2,1,0:T(8,128)(2,1)} %param.13) | copy-start | bytes 12292
  10.5 7.3 %copy-start.6 = (f32[4,8]{1,0:T(4,128)S(1)}, f32[4,8]{1,0:T(4,128)}, u32[]{:S(2)}) copy-start(f32[4,8]{1,0:T(4,128)} %param.17) | copy-start | bytes 388
  11.5 17.9 %copy-start.2 = (bf16[4,8,64,128]{3,2,1,0:T(8,128)(2,1)S(1)}, bf16[4,8,64,128]{3,2,1,0:T(8,128)(2,1)}, u32[]{:S(2)}) copy-start(bf16[4,8,64,128]{3,2,1,0:T(8,128)(2,1)} %param.11) | copy-start | bytes 1572868
  11.5 18.0 %copy-start.4 = (bf16[4,8,64,128]{3,2,1,0:T(8,128)(2,1)S(1)}, bf16[4,8,64,128]{3,2,1,0:T(8,128)(2,1)}, u32[]{:S(2)}) copy-start(bf16[4,8,64,128]{3,2,1,0:T(8,128)(2,1)} %param.10) | copy-start | bytes 1572868
  11.6 3.9 %collective-permute-start = (f32[1,32,146]{2,1,0:T(8,128)S(1)}, f32[1,32,146]{2,1,0:T(8,128)S(1)}, u32[]{:S(2)}, u32[]{:S(2)}) collective-permute-start(f32[1,32,146]{2,1,0:T(8,128)S(1)} %bitcast.215), channel_id=1, source_target_pairs={{0,4},{4,0},{8,12},{12,8},{16,20},{20,16},{24,28},{28,24},{1,5},{5... | collective-permute-start | bytes 56072 | tf_op jit(solution)/shard_map/ppermute | solution.py:12
  13.1 17.2 %collective-permute-start.3 = (bf16[32,4,16,128]{3,2,0,1:T(8,128)(2,1)}, bf16[32,4,16,128]{3,2,0,1:T(8,128)(2,1)S(1)}, u32[]{:S(2)}, u32[]{:S(2)}) collective-permute-start(bf16[32,4,16,128]{3,2,0,1:T(8,128)(2,1)} %fusion.49), channel_id=1, source_target_pairs={{0,4},{4,0},{8,12},{12,8},{16,20},{20,16},{24,28},{28,24},{1,5},{5... | collective-permute-start | bytes 1572872 | tf_op jit(solution)/shard_map/ppermute | solution.py:12
  15.5 4.3 %collective-permute-start.1 = (f32[2,32,146]{2,1,0:T(8,128)S(1)}, f32[2,32,146]{2,1,0:T(8,128)S(1)}, u32[]{:S(2)}, u32[]{:S(2)}) collective-permute-start(f32[2,32,146]{2,1,0:T(8,128)S(1)} %pad_maximum_fusion.3), channel_id=1, source_target_pairs={{0,8},{4,12},{8,0},{12,4},{16,24},{20,28},{24,16},{28,20},{1,9},{5... | collective-permute-start | bytes 112136 | tf_op jit(solution)/shard_map/ppermute | solution.py:12
  19.9 7.8 %collective-permute-start.2 = (f32[4,32,146]{2,1,0:T(8,128)S(1)}, f32[4,32,146]{2,1,0:T(8,128)S(1)}, u32[]{:S(2)}, u32[]{:S(2)}) collective-permute-start(f32[4,32,146]{2,1,0:T(8,128)S(1)} %pad_maximum_fusion.2), channel_id=1, source_target_pairs={{0,16},{4,20},{8,24},{12,28},{16,0},{20,4},{24,8},{28,12},{1,17},{... | collective-permute-start | bytes 224264 | tf_op jit(solution)/shard_map/ppermute | solution.py:12
  30.2 12.6 %copy-start.3 = (f32[4,8,16,128]{3,2,1,0:T(8,128)S(1)}, f32[4,8,16,128]{3,2,1,0:T(8,128)}, u32[]{:S(2)}) copy-start(f32[4,8,16,128]{3,2,1,0:T(8,128)} %param.15) | copy-start | bytes 786436
  30.6 8.3 %collective-permute-start.4 = (bf16[32,16,128]{2,1,0:T(8,128)(2,1)S(1)}, bf16[32,16,128]{2,1,0:T(8,128)(2,1)S(1)}, u32[]{:S(2)}, u32[]{:S(2)}) collective-permute-start(bf16[32,16,128]{2,1,0:T(8,128)(2,1)S(1)} %get-tuple-element.38), channel_id=1, source_target_pairs={{0,8},{4,12},{8,16},{12,20},{16,24},{20,28},{24,0},{28,4},{1,9},{5... | collective-permute-start | bytes 393224 | tf_op jit(solution)/shard_map/ppermute | solution.py:12
  31.3 11.4 %collective-permute-start.5 = (bf16[32,16,128]{2,1,0:T(8,128)(2,1)S(1)}, bf16[32,16,128]{2,1,0:T(8,128)(2,1)S(1)}, u32[]{:S(2)}, u32[]{:S(2)}) collective-permute-start(bf16[32,16,128]{2,1,0:T(8,128)(2,1)S(1)} %get-tuple-element.37), channel_id=1, source_target_pairs={{0,16},{4,20},{8,24},{12,28},{16,0},{20,4},{24,8},{28,12},{1,17},{... | collective-permute-start | bytes 393224 | tf_op jit(solution)/shard_map/ppermute | solution.py:12
  34.7 8.1 %collective-permute-start.6 = (bf16[32,16,128]{2,1,0:T(8,128)(2,1)S(1)}, bf16[32,16,128]{2,1,0:T(8,128)(2,1)S(1)}, u32[]{:S(2)}, u32[]{:S(2)}) collective-permute-start(bf16[32,16,128]{2,1,0:T(8,128)(2,1)S(1)} %get-tuple-element.36), channel_id=1, source_target_pairs={{0,24},{4,28},{8,0},{12,4},{16,8},{20,12},{24,16},{28,20},{1,25},{... | collective-permute-start | bytes 393224 | tf_op jit(solution)/shard_map/ppermute | solution.py:12
  43.2 7.0 %collective-permute-start.7 = (bf16[32,16,128]{2,1,0:T(8,128)(2,1)S(1)}, bf16[32,16,128]{2,1,0:T(8,128)(2,1)S(1)}, u32[]{:S(2)}, u32[]{:S(2)}) collective-permute-start(bf16[32,16,128]{2,1,0:T(8,128)(2,1)S(1)} %get-tuple-element.32), channel_id=1, source_target_pairs={{0,24},{4,28},{8,0},{12,4},{16,8},{20,12},{24,16},{28,20},{1,25},{... | collective-permute-start | bytes 393224 | tf_op jit(solution)/shard_map/ppermute | solution.py:12
  46.6 13.2 %collective-permute-start.8 = (bf16[32,16,128]{2,1,0:T(8,128)(2,1)S(1)}, bf16[32,16,128]{2,1,0:T(8,128)(2,1)S(1)}, u32[]{:S(2)}, u32[]{:S(2)}) collective-permute-start(bf16[32,16,128]{2,1,0:T(8,128)(2,1)S(1)} %get-tuple-element.30), channel_id=1, source_target_pairs={{0,16},{4,20},{8,24},{12,28},{16,0},{20,4},{24,8},{28,12},{1,17},{... | collective-permute-start | bytes 393224 | tf_op jit(solution)/shard_map/ppermute | solution.py:12
  48.3 11.5 %collective-permute-start.9 = (bf16[32,16,128]{2,1,0:T(8,128)(2,1)S(1)}, bf16[32,16,128]{2,1,0:T(8,128)(2,1)S(1)}, u32[]{:S(2)}, u32[]{:S(2)}) collective-permute-start(bf16[32,16,128]{2,1,0:T(8,128)(2,1)S(1)} %get-tuple-element.31), channel_id=1, source_target_pairs={{0,8},{4,12},{8,16},{12,20},{16,24},{20,28},{24,0},{28,4},{1,9},{5... | collective-permute-start | bytes 393224 | tf_op jit(solution)/shard_map/ppermute | solution.py:12
  60.4 13.2 %collective-permute-start.10 = (bf16[32,4,16,128]{3,2,0,1:T(8,128)(2,1)S(1)}, bf16[32,4,16,128]{3,2,0,1:T(8,128)(2,1)S(1)}, u32[]{:S(2)}, u32[]{:S(2)}) collective-permute-start(bf16[32,4,16,128]{3,2,0,1:T(8,128)(2,1)S(1)} %fusion.42), channel_id=1, source_target_pairs={{0,4},{4,0},{8,12},{12,8},{16,20},{20,16},{24,28},{28,24},{1,5},{5... | collective-permute-start | bytes 1572872 | tf_op jit(solution)/shard_map/ppermute | solution.py:12
  62.3 19.9 %collective-permute-start.13 = (bf16[1024,1024]{1,0:T(8,128)(2,1)}, bf16[1024,1024]{1,0:T(8,128)(2,1)S(1)}, u32[]{:S(2)}, u32[]{:S(2)}) collective-permute-start(bf16[1024,1024]{1,0:T(8,128)(2,1)} %collective-permute-done.12), channel_id=1, source_target_pairs={{0,1},{1,0},{2,3},{3,2},{4,5},{5,4},{6,7},{7,6},{8,9},{9,8},{10,11... | collective-permute-start | bytes 6291464 | tf_op jit(solution)/shard_map/ppermute | solution.py:12
  74.5 1.0 %copy-start.9 = (f32[8,128]{1,0:T(8,128)S(1)}, f32[8,128]{1,0:T(8,128)}, u32[]{:S(2)}) copy-start(f32[8,128]{1,0:T(8,128)} %param.18) | copy-start | bytes 12292
  75.3 1.6 %copy-start.8 = (bf16[1024,1024]{1,0:T(8,128)(2,1)S(1)}, bf16[1024,1024]{1,0:T(8,128)(2,1)}, u32[]{:S(2)}) copy-start(bf16[1024,1024]{1,0:T(8,128)(2,1)} %param.19) | copy-start | bytes 6291460
  82.2 1.3 %copy-start.1 = (bf16[4,64,4096]{2,1,0:T(8,128)(2,1)}, bf16[4,64,4096]{2,1,0:T(8,128)(2,1)S(1)}, u32[]{:S(2)}) copy-start(bf16[4,64,4096]{2,1,0:T(8,128)(2,1)S(1)} %fusion.28) | copy-start | bytes 6291460
where the time goes:
time: 85.5 us; the launch traced here: 85.1 us
  waiting for transfers between devices  39.3 us (46%)
  starting transfers between devices  19.6 us (23%)
  matrix products  10.9 us (13%)
  other arithmetic  10.1 us (12%)
  local copies, waits for them, and re-layouts  4.52 us (5%)
    ppermute x14, waiting for transfers between devices, send(): return lax.ppermute(tensor, axis, [(k, move(k)) for k in range(size)])  39.3 us
    ppermute x14, starting transfers between devices, send(): return lax.ppermute(tensor, axis, [(k, move(k)) for k in range(size)])  19.6 us
    dot_general x4, matrix products, on_device(): jnp.einsum('stf,fc->stc', flat, piece, preferred_element_type=jnp.float32)  6.85 us
    unnamed x27, local copies, waits for them, and re-layouts  2.81 us
    dot_general x1, matrix products, cell(): jnp.einsum('psd,pse->pde', weighted.astype(jnp.bfloat16), value, preferre...  2.17 us
  transfers between devices with their start and end apart: 14, of which 9 were waited for; matrix products, arithmetic and copies ran while one was open for 25% of the time, Pallas kernels for 0%

commit v1 on v0

--- a/solution.py
+++ b/solution.py
@@ -34,14 +34,14 @@
 def gather_small(tensor, size):
     me = lax.axis_index("sp")
     whole = tensor[None]
-    bit = 1
-    while bit < size:
+    bit = size // 2
+    while bit > 0:
         other = send(whole, "sp", size, lambda k: k ^ bit)
         upper = (me & bit) != 0
-        whole = jnp.concatenate(
-            [jnp.where(upper, other, whole), jnp.where(upper, whole, other)], axis=0
-        )
-        bit *= 2
+        whole = jnp.stack(
+            [jnp.where(upper, other, whole), jnp.where(upper, whole, other)], axis=1
+        ).reshape((2 * whole.shape[0],) + whole.shape[1:])
+        bit //= 2
     return whole
 
 

time: 85.5 us -> 109 us (1.27)
  other arithmetic: 10.1 us -> 24.3 us
  local copies, waits for them, and re-layouts: 4.52 us -> 12 us
    dynamic_slice x1, other arithmetic: 0.02 us -> 1.78 us  [pick(): return lax.dynamic_index_in_dim(tensor, index, 0, keepdims=False)]
    another operation x1, local copies, waits for them, and re-layouts: 0.13 us -> 1.45 us  [cell(): totals = jnp.cumsum(gathered[:, :, head_width + rows], axis=0)]
    sub x1, other arithmetic: 0.01 us -> 1.28 us  [cell(): own_level = gathered[:, :, head_width + rows + 1] - totals]
    concatenate x1, other arithmetic: 0.01 us -> 1.28 us  [cell(): before = jnp.concatenate([level[None], after[:-1]], axis=0)]
    another operation x1, other arithmetic: 0.02 us -> 1.29 us  [cell(): totals = jnp.cumsum(gathered[:, :, head_width + rows], axis=0)]
    another operation x1, other arithmetic: 0.03 us -> 1.29 us  [cell(): after = jnp.maximum(lax.cummax(own_level, axis=0), level[None])]
    max x1, other arithmetic: 0.01 us -> 1.27 us  [cell(): after = jnp.maximum(lax.cummax(own_level, axis=0), level[None])]
    slice x1, local copies, waits for them, and re-layouts: 0.02 us -> 1.26 us  [cell(): even_before = before[0::2]]
  transfers between devices with their start and end apart: 14 -> 14, of which waited for: 9 -> 8; matrix products, arithmetic and copies ran while one was open for 25% -> 40% of each run, Pallas kernels for 0% -> 0%
where the time goes in v1:
time: 109 us; the launch traced here: 108 us
  waiting for transfers between devices  39 us (36%)
  other arithmetic  24.3 us (22%)
  starting transfers between devices  20.5 us (19%)
  local copies, waits for them, and re-layouts  12 us (11%)
  matrix products  11.7 us (11%)
    ppermute x14, waiting for transfers between devices, send(): return lax.ppermute(tensor, axis, [(k, move(k)) for k in range(size)])  39 us
    ppermute x14, starting transfers between devices, send(): return lax.ppermute(tensor, axis, [(k, move(k)) for k in range(size)])  20.5 us
    dot_general x4, matrix products, on_device(): jnp.einsum('stf,fc->stc', flat, piece, preferred_element_type=jnp.float32)  6.88 us
    unnamed x33, local copies, waits for them, and re-layouts  3.3 us
  transfers between devices with their start and end apart: 14, of which 8 were waited for; matrix products, arithmetic and copies ran while one was open for 40% of the time, Pallas kernels for 0%

profile of v1, /device:TPU:0, one launch (start us, length us, event | category | flops | bytes accessed | tf_op | source)
XLA Modules:
  0.0 108.1 jit_solution(7242492819800599516)
XLA Ops:
  0.0 0.5 collective-permute-start.11
  0.5 2.6 %collective-permute-start.12 = (bf16[1024,1024]{1,0:T(8,128)(2,1)}, bf16[1024,1024]{1,0:T(8,128)(2,1)}, u32[]{:S(2)}, u32[]{:S(2)}) collective-permute-start(bf16[1024,1024]{1,0:T(8,128)(2,1)} %param.19), channel_id=1, source_target_pairs={{0,2},{1,3},{2,0},{3,1},{4,6},{5,7},{6,4},{7,5},{8,10},{9,11},{10,... | collective-permute-start | bytes 6291464 | tf_op jit(solution)/shard_map/ppermute | solution.py:12
  3.1 0.7 fusion.78
  4.3 0.9 fusion.86
  5.2 0.8 subtract_exponential_fusion
  6.1 0.8 subtract_exponential_fusion.1
  6.9 1.4 %multiply_reduce_fusion.1 = f32[4,8,128]{2,1,0:T(8,128)S(1)} fusion(bf16[4,8,64,128]{3,2,1,0:T(8,128)(2,1)} %param.11, f32[4,8,64]{2,1,0:T(8,128)S(1)} %subtract_exponential_fusion), kind=kLoop, calls=%fused_computation.34 | loop fusion | flops 782336 | bytes 548864 | tf_op jit(solution)/shard_map/reduce_sum | solution.py:68
  8.3 2.2 %convolution_convert_fusion = bf16[32,128,128]{2,1,0:T(8,128)(2,1)S(1)} fusion(bf16[32,64,128]{2,1,0:T(8,128)(2,1)S(1)} %bitcast.229, bf16[32,64,128]{2,1,0:T(8,128)(2,1)} %bitcast.236, f32[32,64]{1,0:T(8,128)S(1)} %subtract_exponential_fusion.1), kind=kOutput, calls=%fused_computation.8 | convolution fusion | flops 68419584 | bytes 2105344 | tf_op jit(solution)/shard_map/psd,pse->pde/dot_general | solution.py:72
  10.7 0.5 copy-done.10
  11.3 2.6 %collective-permute-start = (f32[1,32,146]{2,1,0:T(8,128)S(1)}, f32[1,32,146]{2,1,0:T(8,128)S(1)}, u32[]{:S(2)}, u32[]{:S(2)}) collective-permute-start(f32[1,32,146]{2,1,0:T(8,128)S(1)} %bitcast.242), channel_id=1, source_target_pairs={{0,16},{4,20},{8,24},{12,28},{16,0},{20,4},{24,8},{28,12},{1,17},{... | collective-permute-start | bytes 56072 | tf_op jit(solution)/shard_map/ppermute | solution.py:12
  13.8 1.5 %collective-permute-start.3 = (bf16[32,4,16,128]{3,2,0,1:T(8,128)(2,1)S(1)}, bf16[32,4,16,128]{3,2,0,1:T(8,128)(2,1)S(1)}, u32[]{:S(2)}, u32[]{:S(2)}) collective-permute-start(bf16[32,4,16,128]{3,2,0,1:T(8,128)(2,1)S(1)} %fusion.49), channel_id=1, source_target_pairs={{0,4},{4,0},{8,12},{12,8},{16,20},{20,16},{24,28},{28,24},{1,5},{5... | collective-permute-start | bytes 1572872 | tf_op jit(solution)/shard_map/ppermute | solution.py:12
  15.4 1.0 collective-permute-done
  16.5 1.3 %collective-permute-start.1 = (f32[2,32,146]{2,1,0:T(8,128)S(1)}, f32[2,32,146]{2,1,0:T(8,128)S(1)}, u32[]{:S(2)}, u32[]{:S(2)}) collective-permute-start(f32[2,32,146]{2,1,0:T(8,128)S(1)} %maximum_bitcast_fusion), channel_id=1, source_target_pairs={{0,8},{4,12},{8,0},{12,4},{16,24},{20,28},{24,16},{28,20},{1,9},{5... | collective-permute-start | bytes 112136 | tf_op jit(solution)/shard_map/ppermute | solution.py:12
  17.7 1.2 %fusion.41 = f32[32,64]{1,0:T(8,128)} fusion(f32[32,64]{1,0:T(8,128)S(1)} %convert_bitcast_fusion, f32[32,64]{1,0:T(8,128)S(1)} %reduce_window_sum.26, pred[64,64]{0,1:T(8,128)(4,1)S(1)} %iota_compare_fusion), kind=kLoop, calls=%fused_computation.37 | loop fusion | flops 522240 | bytes 28672 | tf_op jit(solution)/shard_map/reduce_max | solution.py:158
  19.0 0.6 max.45
  19.6 0.6 broadcast_in_dim_reshape.4
  20.3 0.5 collective-permute-done.1
  20.8 1.6 %collective-permute-start.2 = (f32[4,32,146]{2,1,0:T(8,128)S(1)}, f32[4,32,146]{2,1,0:T(8,128)S(1)}, u32[]{:S(2)}, u32[]{:S(2)}) collective-permute-start(f32[4,32,146]{2,1,0:T(8,128)S(1)} %bitcast.239), channel_id=1, source_target_pairs={{0,4},{4,0},{8,12},{12,8},{16,20},{20,16},{24,28},{28,24},{1,5},{5... | collective-permute-start | bytes 224264 | tf_op jit(solution)/shard_map/ppermute | solution.py:12
  22.4 0.5 iota_compare_fusion.1
  22.9 7.5 %collective-permute-done.2 = f32[4,32,146]{2,1,0:T(8,128)S(1)} collective-permute-done((f32[4,32,146]{2,1,0:T(8,128)S(1)}, f32[4,32,146]{2,1,0:T(8,128)S(1)}, u32[]{:S(2)}, u32[]{:S(2)}) %collective-permute-start.2) | collective-permute-done | bytes 74784 | tf_op jit(solution)/shard_map/ppermute | solution.py:12
  30.4 0.9 slice_reduce_fusion.1
  31.3 1.3 %reduce_window_sum.28 = f32[8,32]{1,0:T(8,128)} reduce-window(f32[8,32]{1,0:T(8,128)} %get-tuple-element.10, f32[]{:T(128)} %constant.204.clone.1), window={size=8x1 pad=7_0x0_0}, to_apply=%region_3.4 | reduce-window | flops 1792 | bytes 2052 | tf_op jit(solution)/shard_map/jit(cumsum)/reduce_window_sum | solution.py:90
  32.6 1.5 %copy.106 = f32[8,32,1]{2,1,0:T(8,128)} copy(f32[8,32,1]{1,0,2:T(8,128)} %bitcast.244) | data formatting | bytes 2048 | tf_op jit(solution)/shard_map/jit(cumsum)/reduce_window_sum | solution.py:90
  34.1 1.3 %sub.306 = f32[8,32]{1,0:T(8,128)} subtract(f32[8,32]{1,0:T(8,128)} %get-tuple-element.9, f32[8,32]{1,0:T(8,128)} %reduce_window_sum.28) | non-fusion elementwise | flops 256 | bytes 3072 | tf_op jit(solution)/shard_map/sub | solution.py:91
  35.3 1.3 %reduce_window_max.10 = f32[8,32]{1,0:T(8,128)} reduce-window(f32[8,32]{1,0:T(8,128)} %sub.306, f32[]{:T(128)} %constant.212.clone.1), window={size=8x1 pad=7_0x0_0}, to_apply=%region_4.5 | reduce-window | flops 1792 | bytes 2052 | tf_op jit(solution)/shard_map/cell/reduce_window_max | solution.py:92
  36.6 1.3 %broadcast_maximum_fusion = f32[8,32]{1,0:T(8,128)} fusion(f32[8,32]{1,0:T(8,128)} %reduce_window_max.10, f32[32]{0:T(128)} %max.45), kind=kLoop, calls=%fused_computation.166 | loop fusion | flops 256 | bytes 2176 | tf_op jit(solution)/shard_map/max | solution.py:92
  37.9 1.3 %slice.40 = f32[4,32]{1,0:T(4,128)} slice(f32[8,32]{1,0:T(8,128)} %broadcast_maximum_fusion), slice={[1:8:2], [0:32:1]} | slice | bytes 1024 | tf_op jit(solution)/shard_map/slice | solution.py:95
  39.1 1.3 %pad_maximum_fusion.4 = f32[8,32]{1,0:T(8,128)} fusion(f32[7,32]{1,0:T(8,128)} %bitcast.245, f32[1,32]{1,0:T(1,128)} %broadcast_in_dim_reshape.4), kind=kLoop, calls=%fused_computation.164 | loop fusion | flops 256 | bytes 2048 | tf_op jit(solution)/shard_map/concatenate | solution.py:93
  40.4 1.3 %slice.39 = f32[4,32]{1,0:T(4,128)} slice(f32[8,32]{1,0:T(8,128)} %pad_maximum_fusion.4), slice={[0:8:2], [0:32:1]} | slice | bytes 1024 | tf_op jit(solution)/shard_map/slice | solution.py:94
  41.7 1.8 %fusion.104 = (f32[32]{0:T(128)}, f32[32]{0:T(128)S(1)}, f32[32,1]{0,1:T(1,128)}) fusion(f32[8,32]{1,0:T(8,128)} %pad_maximum_fusion.4, s32[]{:T(128)S(6)} %select_n.415, f32[8,32]{1,0:T(8,128)} %reduce_window_sum.28), kind=kLoop, calls=%fused_computation.206 | loop fusion | flops 32 | bytes 644 | tf_op jit(solution)/shard_map/jit(dynamic_index_in_dim)/dynamic_slice | solution.py:49
  43.5 1.1 %select_reduce_fusion = f32[8,32]{1,0:T(8,128)S(1)} fusion(f32[8,32,1]{2,1,0:T(8,128)} %copy.106, f32[8,32,146]{2,1,0:T(8,128)S(1)} %bitcast.234, f32[32]{0:T(128)S(1)} %get-tuple-element.50, pred[8]{0:T(512)(128)(4,1)} %iota_compare_fusion.1), kind=kLoop, calls=%fused_computation.113 | loop fusion | flops 1024 | bytes 3208 | tf_op jit(solution)/shard_map/jit(_where)/select_n | solution.py:146
  44.6 0.7 fusion.77
  45.3 0.7 squeeze.84
  46.0 0.7 subtract_exponential_fusion.2
  46.7 0.7 copy.96
  47.6 0.8 add_maximum_fusion
  48.4 0.8 subtract_exponential_fusion.4
  49.2 0.8 broadcast_select_fusion.6
  50.1 0.8 fusion.102
  51.1 0.8 bitcast_add_fusion
  51.9 1.5 %fusion.114 = (f32[32,64]{1,0:T(8,128)S(1)}, bf16[32,64,64]{1,2,0:T(8,128)(2,1)S(1)}) fusion(f32[32,64]{1,0:T(8,128)S(1)} %add_maximum_fusion, f32[32,64]{1,0:T(8,128)} %copy-done.7, f32[32,64]{1,0:T(8,128)S(1)} %reduce_window_sum.26, pred[64,64]{0,1:T(8,128)(4,1)} %copy-done.8, bf16[32,64,128]{2,1,0:T(8,128)(2,1)S(1)} %bitcast.240, ...), kind=kOutput, calls=%fused_computation.209 | convolution fusion | flops 34600960 | bytes 1347584 | tf_op jit(solution)/shard_map/ptd,psd->pts/dot_general | solution.py:160
  53.8 1.6 %collective-permute-start.4 = (bf16[32,16,128]{2,1,0:T(8,128)(2,1)S(1)}, bf16[32,16,128]{2,1,0:T(8,128)(2,1)S(1)}, u32[]{:S(2)}, u32[]{:S(2)}) collective-permute-start(bf16[32,16,128]{2,1,0:T(8,128)(2,1)S(1)} %get-tuple-element.38), channel_id=1, source_target_pairs={{0,8},{4,12},{8,16},{12,20},{16,24},{20,28},{24,0},{28,4},{1,9},{5... | collective-permute-start | bytes 393224 | tf_op jit(solution)/shard_map/ppermute | solution.py:12
  55.4 0.4 collective-permute-start.5
  55.8 2.1 %collective-permute-start.6 = (bf16[32,16,128]{2,1,0:T(8,128)(2,1)S(1)}, bf16[32,16,128]{2,1,0:T(8,128)(2,1)S(1)}, u32[]{:S(2)}, u32[]{:S(2)}) collective-permute-start(bf16[32,16,128]{2,1,0:T(8,128)(2,1)S(1)} %get-tuple-element.36), channel_id=1, source_target_pairs={{0,24},{4,28},{8,0},{12,4},{16,8},{20,12},{24,16},{28,20},{1,25},{... | collective-permute-start | bytes 393224 | tf_op jit(solution)/shard_map/ppermute | solution.py:12
  57.9 4.2 %collective-permute-done.4 = bf16[32,16,128]{2,1,0:T(8,128)(2,1)S(1)} collective-permute-done((bf16[32,16,128]{2,1,0:T(8,128)(2,1)S(1)}, bf16[32,16,128]{2,1,0:T(8,128)(2,1)S(1)}, u32[]{:S(2)}, u32[]{:S(2)}) %collective-permute-start.4) | collective-permute-done | bytes 131104 | tf_op jit(solution)/shard_map/ppermute | solution.py:12
  62.0 3.8 %collective-permute-done.5 = bf16[32,16,128]{2,1,0:T(8,128)(2,1)S(1)} collective-permute-done((bf16[32,16,128]{2,1,0:T(8,128)(2,1)S(1)}, bf16[32,16,128]{2,1,0:T(8,128)(2,1)S(1)}, u32[]{:S(2)}, u32[]{:S(2)}) %collective-permute-start.5) | collective-permute-done | bytes 131104 | tf_op jit(solution)/shard_map/ppermute | solution.py:12
  65.9 0.4 fusion.68
  66.3 3.3 %collective-permute-start.7 = (bf16[32,16,128]{2,1,0:T(8,128)(2,1)S(1)}, bf16[32,16,128]{2,1,0:T(8,128)(2,1)S(1)}, u32[]{:S(2)}, u32[]{:S(2)}) collective-permute-start(bf16[32,16,128]{2,1,0:T(8,128)(2,1)S(1)} %get-tuple-element.32), channel_id=1, source_target_pairs={{0,24},{4,28},{8,0},{12,4},{16,8},{20,12},{24,16},{28,20},{1,25},{... | collective-permute-start | bytes 393224 | tf_op jit(solution)/shard_map/ppermute | solution.py:12
  69.6 0.4 fusion.72
  70.0 1.5 %collective-permute-start.8 = (bf16[32,16,128]{2,1,0:T(8,128)(2,1)S(1)}, bf16[32,16,128]{2,1,0:T(8,128)(2,1)S(1)}, u32[]{:S(2)}, u32[]{:S(2)}) collective-permute-start(bf16[32,16,128]{2,1,0:T(8,128)(2,1)S(1)} %get-tuple-element.30), channel_id=1, source_target_pairs={{0,16},{4,20},{8,24},{12,28},{16,0},{20,4},{24,8},{28,12},{1,17},{... | collective-permute-start | bytes 393224 | tf_op jit(solution)/shard_map/ppermute | solution.py:12
  71.5 1.8 %collective-permute-done.7 = bf16[32,16,128]{2,1,0:T(8,128)(2,1)S(1)} collective-permute-done((bf16[32,16,128]{2,1,0:T(8,128)(2,1)S(1)}, bf16[32,16,128]{2,1,0:T(8,128)(2,1)S(1)}, u32[]{:S(2)}, u32[]{:S(2)}) %collective-permute-start.7) | collective-permute-done | bytes 131104 | tf_op jit(solution)/shard_map/ppermute | solution.py:12
  73.3 9.6 %collective-permute-done.8 = bf16[32,16,128]{2,1,0:T(8,128)(2,1)S(1)} collective-permute-done((bf16[32,16,128]{2,1,0:T(8,128)(2,1)S(1)}, bf16[32,16,128]{2,1,0:T(8,128)(2,1)S(1)}, u32[]{:S(2)}, u32[]{:S(2)}) %collective-permute-start.8) | collective-permute-done | bytes 131104 | tf_op jit(solution)/shard_map/ppermute | solution.py:12
  83.1 0.4 fusion.42
  83.5 1.5 %collective-permute-start.10 = (bf16[32,4,16,128]{3,2,0,1:T(8,128)(2,1)S(1)}, bf16[32,4,16,128]{3,2,0,1:T(8,128)(2,1)S(1)}, u32[]{:S(2)}, u32[]{:S(2)}) collective-permute-start(bf16[32,4,16,128]{3,2,0,1:T(8,128)(2,1)S(1)} %fusion.42), channel_id=1, source_target_pairs={{0,4},{4,0},{8,12},{12,8},{16,20},{20,16},{24,28},{28,24},{1,5},{5... | collective-permute-start | bytes 1572872 | tf_op jit(solution)/shard_map/ppermute | solution.py:12
  85.4 0.3 fusion.50
  85.9 10.6 %collective-permute-done.10 = bf16[32,4,16,128]{3,2,0,1:T(8,128)(2,1)S(1)} collective-permute-done((bf16[32,4,16,128]{3,2,0,1:T(8,128)(2,1)S(1)}, bf16[32,4,16,128]{3,2,0,1:T(8,128)(2,1)S(1)}, u32[]{:S(2)}, u32[]{:S(2)}) %collective-permute-start.10) | collective-permute-done | bytes 524320 | tf_op jit(solution)/shard_map/ppermute | solution.py:12
  96.5 0.5 select_bitcast_fusion.1
  97.5 0.8 fusion.12
  98.5 1.3 %copy-done.11 = bf16[1024,1024]{1,0:T(8,128)(2,1)S(1)} copy-done((bf16[1024,1024]{1,0:T(8,128)(2,1)S(1)}, bf16[1024,1024]{1,0:T(8,128)(2,1)}, u32[]{:S(2)}) %copy-start.11) | copy-done | bytes 2097176
  99.8 0.7 fusion.34
  100.6 2.3 %fusion.31 = bf16[4,64,4096]{2,1,0:T(8,128)(2,1)S(1)} fusion(bf16[4,64,4096]{2,1,0:T(8,128)(2,1)S(1)} %fusion.34, s32[]{:T(128)S(6)} %select_n.477, bf16[1024,1024]{1,0:T(8,128)(2,1)} %collective-permute-done.11, bf16[4,8,64,128]{3,2,1,0:T(8,128)(2,1)S(1)} %bitcast.248, f32[8,128]{1,0:T(8,128)S(1)} %copy-done.12), kind=kOutput, calls=%fused_computation.24 | convolution fusion | flops 537919488 | bytes 3149828 | tf_op jit(solution)/shard_map/stf,fc->stc/dot_general | solution.py:212
  102.9 2.3 %fusion.28 = bf16[4,64,4096]{2,1,0:T(8,128)(2,1)S(1)} fusion(bf16[4,64,4096]{2,1,0:T(8,128)(2,1)S(1)} %fusion.31, s32[]{:T(128)S(6)} %select_n.479, bf16[1024,1024]{1,0:T(8,128)(2,1)} %collective-permute-done.12, bf16[4,8,64,128]{3,2,1,0:T(8,128)(2,1)S(1)} %bitcast.249, f32[8,128]{1,0:T(8,128)S(1)} %copy-done.12), kind=kOutput, calls=%fused_computation.23 | convolution fusion | flops 537919488 | bytes 3149828 | tf_op jit(solution)/shard_map/stf,fc->stc/dot_general | solution.py:212
  105.3 1.3 %copy-done.1 = bf16[4,64,4096]{2,1,0:T(8,128)(2,1)} copy-done((bf16[4,64,4096]{2,1,0:T(8,128)(2,1)}, bf16[4,64,4096]{2,1,0:T(8,128)(2,1)S(1)}, u32[]{:S(2)}) %copy-start.1) | copy-done | bytes 2097176
  106.6 1.5 %fusion.25 = bf16[4,64,4096]{2,1,0:T(8,128)(2,1)} fusion(bf16[4,64,4096]{2,1,0:T(8,128)(2,1)} %copy-done.1, s32[]{:T(128)S(6)} %select_n.480, bf16[1024,1024]{1,0:T(8,128)(2,1)S(1)} %collective-permute-done.13, bf16[4,8,64,128]{3,2,1,0:T(8,128)(2,1)S(1)} %bitcast.250, f32[8,128]{1,0:T(8,128)S(1)} %copy-done.12), kind=kOutput, calls=%fused_computation.22 | convolution fusion | flops 537919488 | bytes 3149828 | tf_op jit(solution)/shard_map/stf,fc->stc/dot_general | solution.py:212
  (70 shorter events, 3.2 us)
Async XLA Ops:
  0.0 8.3 %copy-start = (bf16[4,8,64,128]{3,2,1,0:T(8,128)(2,1)S(1)}, bf16[4,8,64,128]{3,2,1,0:T(8,128)(2,1)}, u32[]{:S(2)}) copy-start(bf16[4,8,64,128]{3,2,1,0:T(8,128)(2,1)} %param.12) | copy-start | bytes 1572868
  0.0 100.6 %collective-permute-start.11 = (bf16[1024,1024]{1,0:T(8,128)(2,1)}, bf16[1024,1024]{1,0:T(8,128)(2,1)}, u32[]{:S(2)}, u32[]{:S(2)}) collective-permute-start(bf16[1024,1024]{1,0:T(8,128)(2,1)} %param.19), channel_id=1, source_target_pairs={{0,1},{1,0},{2,3},{3,2},{4,5},{5,4},{6,7},{7,6},{8,9},{9,8},{10,11... | collective-permute-start | bytes 6291464 | tf_op jit(solution)/shard_map/ppermute | solution.py:12
  0.5 85.2 %collective-permute-start.12 = (bf16[1024,1024]{1,0:T(8,128)(2,1)}, bf16[1024,1024]{1,0:T(8,128)(2,1)}, u32[]{:S(2)}, u32[]{:S(2)}) collective-permute-start(bf16[1024,1024]{1,0:T(8,128)(2,1)} %param.19), channel_id=1, source_target_pairs={{0,2},{1,3},{2,0},{3,1},{4,6},{5,7},{6,4},{7,5},{8,10},{9,11},{10,... | collective-permute-start | bytes 6291464 | tf_op jit(solution)/shard_map/ppermute | solution.py:12
  10.5 0.7 copy-start.10
  10.5 4.9 %copy-start.6 = (bf16[4,8,64]{2,1,0:T(8,128)(2,1)S(1)}, bf16[4,8,64]{2,1,0:T(8,128)(2,1)}, u32[]{:S(2)}) copy-start(bf16[4,8,64]{2,1,0:T(8,128)(2,1)} %param.13) | copy-start | bytes 12292
  10.5 8.5 %copy-start.9 = (f32[4,8]{1,0:T(4,128)S(1)}, f32[4,8]{1,0:T(4,128)}, u32[]{:S(2)}) copy-start(f32[4,8]{1,0:T(4,128)} %param.17) | copy-start | bytes 388
  11.3 5.2 %collective-permute-start = (f32[1,32,146]{2,1,0:T(8,128)S(1)}, f32[1,32,146]{2,1,0:T(8,128)S(1)}, u32[]{:S(2)}, u32[]{:S(2)}) collective-permute-start(f32[1,32,146]{2,1,0:T(8,128)S(1)} %bitcast.242), channel_id=1, source_target_pairs={{0,16},{4,20},{8,24},{12,28},{16,0},{20,4},{24,8},{28,12},{1,17},{... | collective-permute-start | bytes 56072 | tf_op jit(solution)/shard_map/ppermute | solution.py:12
  13.8 39.6 %collective-permute-start.3 = (bf16[32,4,16,128]{3,2,0,1:T(8,128)(2,1)S(1)}, bf16[32,4,16,128]{3,2,0,1:T(8,128)(2,1)S(1)}, u32[]{:S(2)}, u32[]{:S(2)}) collective-permute-start(bf16[32,4,16,128]{3,2,0,1:T(8,128)(2,1)S(1)} %fusion.49), channel_id=1, source_target_pairs={{0,4},{4,0},{8,12},{12,8},{16,20},{20,16},{24,28},{28,24},{1,5},{5... | collective-permute-start | bytes 1572872 | tf_op jit(solution)/shard_map/ppermute | solution.py:12
  15.3 4.9 %copy-start.7 = (f32[32,64]{1,0:T(8,128)}, f32[32,64]{1,0:T(8,128)S(1)}, u32[]{:S(2)}) copy-start(f32[32,64]{1,0:T(8,128)S(1)} %convert_bitcast_fusion) | copy-start | bytes 24580
  15.4 4.9 %copy-start.8 = (pred[64,64]{0,1:T(8,128)(4,1)}, pred[64,64]{0,1:T(8,128)(4,1)S(1)}, u32[]{:S(2)}) copy-start(pred[64,64]{0,1:T(8,128)(4,1)S(1)} %iota_compare_fusion) | copy-start | bytes 12292
  16.5 4.3 %collective-permute-start.1 = (f32[2,32,146]{2,1,0:T(8,128)S(1)}, f32[2,32,146]{2,1,0:T(8,128)S(1)}, u32[]{:S(2)}, u32[]{:S(2)}) collective-permute-start(f32[2,32,146]{2,1,0:T(8,128)S(1)} %maximum_bitcast_fusion), channel_id=1, source_target_pairs={{0,8},{4,12},{8,0},{12,4},{16,24},{20,28},{24,16},{28,20},{1,9},{5... | collective-permute-start | bytes 112136 | tf_op jit(solution)/shard_map/ppermute | solution.py:12
  20.2 31.6 %copy-start.2 = (bf16[4,8,64,128]{3,2,1,0:T(8,128)(2,1)S(1)}, bf16[4,8,64,128]{3,2,1,0:T(8,128)(2,1)}, u32[]{:S(2)}) copy-start(bf16[4,8,64,128]{3,2,1,0:T(8,128)(2,1)} %param.11) | copy-start | bytes 1572868
  20.2 31.6 %copy-start.4 = (bf16[4,8,64,128]{3,2,1,0:T(8,128)(2,1)S(1)}, bf16[4,8,64,128]{3,2,1,0:T(8,128)(2,1)}, u32[]{:S(2)}) copy-start(bf16[4,8,64,128]{3,2,1,0:T(8,128)(2,1)} %param.10) | copy-start | bytes 1572868
  20.8 9.5 %collective-permute-start.2 = (f32[4,32,146]{2,1,0:T(8,128)S(1)}, f32[4,32,146]{2,1,0:T(8,128)S(1)}, u32[]{:S(2)}, u32[]{:S(2)}) collective-permute-start(f32[4,32,146]{2,1,0:T(8,128)S(1)} %bitcast.239), channel_id=1, source_target_pairs={{0,4},{4,0},{8,12},{12,8},{16,20},{20,16},{24,28},{28,24},{1,5},{5... | collective-permute-start | bytes 224264 | tf_op jit(solution)/shard_map/ppermute | solution.py:12
  53.4 12.5 %copy-start.3 = (f32[4,8,16,128]{3,2,1,0:T(8,128)S(1)}, f32[4,8,16,128]{3,2,1,0:T(8,128)}, u32[]{:S(2)}) copy-start(f32[4,8,16,128]{3,2,1,0:T(8,128)} %param.15) | copy-start | bytes 786436
  53.8 8.3 %collective-permute-start.4 = (bf16[32,16,128]{2,1,0:T(8,128)(2,1)S(1)}, bf16[32,16,128]{2,1,0:T(8,128)(2,1)S(1)}, u32[]{:S(2)}, u32[]{:S(2)}) collective-permute-start(bf16[32,16,128]{2,1,0:T(8,128)(2,1)S(1)} %get-tuple-element.38), channel_id=1, source_target_pairs={{0,8},{4,12},{8,16},{12,20},{16,24},{20,28},{24,0},{28,4},{1,9},{5... | collective-permute-start | bytes 393224 | tf_op jit(solution)/shard_map/ppermute | solution.py:12
  55.4 10.5 %collective-permute-start.5 = (bf16[32,16,128]{2,1,0:T(8,128)(2,1)S(1)}, bf16[32,16,128]{2,1,0:T(8,128)(2,1)S(1)}, u32[]{:S(2)}, u32[]{:S(2)}) collective-permute-start(bf16[32,16,128]{2,1,0:T(8,128)(2,1)S(1)} %get-tuple-element.37), channel_id=1, source_target_pairs={{0,16},{4,20},{8,24},{12,28},{16,0},{20,4},{24,8},{28,12},{1,17},{... | collective-permute-start | bytes 393224 | tf_op jit(solution)/shard_map/ppermute | solution.py:12
  55.8 10.1 %collective-permute-start.6 = (bf16[32,16,128]{2,1,0:T(8,128)(2,1)S(1)}, bf16[32,16,128]{2,1,0:T(8,128)(2,1)S(1)}, u32[]{:S(2)}, u32[]{:S(2)}) collective-permute-start(bf16[32,16,128]{2,1,0:T(8,128)(2,1)S(1)} %get-tuple-element.36), channel_id=1, source_target_pairs={{0,24},{4,28},{8,0},{12,4},{16,8},{20,12},{24,16},{28,20},{1,25},{... | collective-permute-start | bytes 393224 | tf_op jit(solution)/shard_map/ppermute | solution.py:12
  66.3 7.0 %collective-permute-start.7 = (bf16[32,16,128]{2,1,0:T(8,128)(2,1)S(1)}, bf16[32,16,128]{2,1,0:T(8,128)(2,1)S(1)}, u32[]{:S(2)}, u32[]{:S(2)}) collective-permute-start(bf16[32,16,128]{2,1,0:T(8,128)(2,1)S(1)} %get-tuple-element.32), channel_id=1, source_target_pairs={{0,24},{4,28},{8,0},{12,4},{16,8},{20,12},{24,16},{28,20},{1,25},{... | collective-permute-start | bytes 393224 | tf_op jit(solution)/shard_map/ppermute | solution.py:12
  70.0 12.9 %collective-permute-start.8 = (bf16[32,16,128]{2,1,0:T(8,128)(2,1)S(1)}, bf16[32,16,128]{2,1,0:T(8,128)(2,1)S(1)}, u32[]{:S(2)}, u32[]{:S(2)}) collective-permute-start(bf16[32,16,128]{2,1,0:T(8,128)(2,1)S(1)} %get-tuple-element.30), channel_id=1, source_target_pairs={{0,16},{4,20},{8,24},{12,28},{16,0},{20,4},{24,8},{28,12},{1,17},{... | collective-permute-start | bytes 393224 | tf_op jit(solution)/shard_map/ppermute | solution.py:12
  71.5 11.4 %collective-permute-start.9 = (bf16[32,16,128]{2,1,0:T(8,128)(2,1)S(1)}, bf16[32,16,128]{2,1,0:T(8,128)(2,1)S(1)}, u32[]{:S(2)}, u32[]{:S(2)}) collective-permute-start(bf16[32,16,128]{2,1,0:T(8,128)(2,1)S(1)} %get-tuple-element.31), channel_id=1, source_target_pairs={{0,8},{4,12},{8,16},{12,20},{16,24},{20,28},{24,0},{28,4},{1,9},{5... | collective-permute-start | bytes 393224 | tf_op jit(solution)/shard_map/ppermute | solution.py:12
  83.1 2.7 %copy-start.5 = (f32[32,64]{1,0:T(8,128)S(1)}, f32[32,64]{1,0:T(8,128)}, u32[]{:S(2)}) copy-start(f32[32,64]{1,0:T(8,128)} %fusion.41) | copy-start | bytes 24580
  83.5 13.1 %collective-permute-start.10 = (bf16[32,4,16,128]{3,2,0,1:T(8,128)(2,1)S(1)}, bf16[32,4,16,128]{3,2,0,1:T(8,128)(2,1)S(1)}, u32[]{:S(2)}, u32[]{:S(2)}) collective-permute-start(bf16[32,4,16,128]{3,2,0,1:T(8,128)(2,1)S(1)} %fusion.42), channel_id=1, source_target_pairs={{0,4},{4,0},{8,12},{12,8},{16,20},{20,16},{24,28},{28,24},{1,5},{5... | collective-permute-start | bytes 1572872 | tf_op jit(solution)/shard_map/ppermute | solution.py:12
  85.7 19.5 %collective-permute-start.13 = (bf16[1024,1024]{1,0:T(8,128)(2,1)}, bf16[1024,1024]{1,0:T(8,128)(2,1)S(1)}, u32[]{:S(2)}, u32[]{:S(2)}) collective-permute-start(bf16[1024,1024]{1,0:T(8,128)(2,1)} %collective-permute-done.12), channel_id=1, source_target_pairs={{0,1},{1,0},{2,3},{3,2},{4,5},{5,4},{6,7},{7,6},{8,9},{9,8},{10,11... | collective-permute-start | bytes 6291464 | tf_op jit(solution)/shard_map/ppermute | solution.py:12
  97.5 1.0 copy-start.12
  98.2 1.6 %copy-start.11 = (bf16[1024,1024]{1,0:T(8,128)(2,1)S(1)}, bf16[1024,1024]{1,0:T(8,128)(2,1)}, u32[]{:S(2)}) copy-start(bf16[1024,1024]{1,0:T(8,128)(2,1)} %param.19) | copy-start | bytes 6291460
  105.2 1.3 %copy-start.1 = (bf16[4,64,4096]{2,1,0:T(8,128)(2,1)}, bf16[4,64,4096]{2,1,0:T(8,128)(2,1)S(1)}, u32[]{:S(2)}) copy-start(bf16[4,64,4096]{2,1,0:T(8,128)(2,1)S(1)} %fusion.28) | copy-start | bytes 6291460
